TPU v7x, 32 devices: a whole 2x2x4 slice. The times are simulated.
32 devices in a mesh: gr: 2 (over core), fs: 8 (over z, y), tp: 2 (over x).
Axes of the slice: x: 2, y: 2, z: 4, core: 2. Of those that a mesh axis runs over, the one named last changes fastest.
Arguments:
- tokens: bfloat16 [2048, 2048], P(('gr', 'fs')), may hold values from -60 to 60
- route_ids: int32 [2048, 2], P(('gr', 'fs')), may hold values from 0 to 7, all different within a row; in each aligned block of 128 rows (0 to 127, 128 to 255, ...) at most 32 rows name the same one
- route_logits: float32 [2048, 2], P(('gr', 'fs')), may hold values from -8 to 8
- norm_gain: float32 [2048], P(('gr', 'fs')), may hold values from 0.1 to 1.9
- gate_master: float32 [8, 2048, 7168], P(None, ('gr', 'fs'), 'tp'), may hold values from -0.125 to 0.125
- up_master: float32 [8, 2048, 7168], P(None, ('gr', 'fs'), 'tp'), may hold values from -0.125 to 0.125
- down_master: float32 [8, 7168, 2048], P(None, 'fs', ('gr', 'tp')), may hold values from -0.0625 to 0.0625
Outputs:
- gate_weight: bfloat16 [8, 2048, 7168], P('tp', None, 'fs')
- up_weight: bfloat16 [8, 2048, 7168], P('tp', None, 'fs')
- down_weight: bfloat16 [8, 7168, 2048], P('tp', 'fs')
- mixed: bfloat16 [2048, 2048], P(('gr', 'fs'))
Inputs may be any that keep to these rules, and one draw needn't show every extreme that they name: `route_ids`: in the rows of one device, that is in each aligned block of 128 rows, each of the 8 experts is named by exactly 32 rows; a row names two different experts.
All inputs are finite; a program needn't handle non-finite values.
Results may differ from a plain program's by a relative error of at most 0.025.
Values may be sent and summed in bfloat16 or wider, within the bound.
A program may use at most 192 MiB of HBM per device.

v0:
```python
import functools

import jax
import jax.numpy as jnp
from jax import lax
from jax.experimental import pallas as pl
from jax.experimental.pallas import tpu as pltpu
from jax.sharding import PartitionSpec as P

CAP = 32


epsilon = 1e-06
MESH = pl.DeviceIdType.MESH
BF16 = jnp.bfloat16


def exchange_kernel(
    n_gr, n_fs, n_tp,
    gain_ref, gate_ref, up_ref, down_ref,
    gate_out, up_out, down_out,
    stage, stage_down, crossed, raw, raw_down,
    load_sem, load_down_sem, x_send, x_recv, s_send, s_recv, own_sem,
    d_send, d_recv, xd_send, xd_recv, own_down_sem, dd_send, dd_recv,
):
    gr, fs, tp = (lax.axis_index(name) for name in ("gr", "fs", "tp"))
    experts, _, width = gate_out.shape
    rows, cols = gate_ref.shape[1], gate_ref.shape[2]
    per = cols // width
    down_cols = down_ref.shape[2]
    masters, outs = (gate_ref, up_ref), (gate_out, up_out)

    barrier = pltpu.get_barrier_semaphore()
    peers = 0
    for o in range(1, n_tp):
        pl.semaphore_signal(barrier, 1, device_id=(gr, fs, lax.rem(tp + o, n_tp)), device_id_type=MESH)
        peers += 1
    for k in range(1, n_fs):
        pl.semaphore_signal(barrier, 1, device_id=(gr, lax.rem(fs + k, n_fs), tp), device_id_type=MESH)
        peers += 1
    for o in range(1, n_gr):
        pl.semaphore_signal(barrier, 1, device_id=(lax.rem(gr + o, n_gr), fs, tp), device_id_type=MESH)
        peers += 1

    def tp_at(o):
        return lax.rem(tp + o, n_tp)

    order = [(w, o) for w in range(2) for o in [*range(1, n_tp), 0]]

    def load(e, w, o):
        return pltpu.make_async_copy(
            masters[w].at[tp_at(o) * experts + e], raw.at[w, o], load_sem.at[w, o]
        )

    def load_down(e, o):
        return pltpu.make_async_copy(
            down_ref.at[tp_at(o) * experts + e], raw_down.at[o], load_down_sem.at[o]
        )

    def over_tp(e, w, o, j):
        columns = pl.ds(j * width, width)
        return pltpu.make_async_remote_copy(
            stage.at[w, o, e, :, columns], crossed.at[w, o - 1, e, :, columns],
            x_send.at[w, o - 1, e, j], x_recv.at[w, o - 1, e, j],
            device_id=(gr, fs, tp_at(o)), device_id_type=MESH,
        )

    def rows_of(group, owner):
        return pl.ds(pl.multiple_of((group * n_fs + owner) * rows, rows), rows)

    def source(e, w, o, j):
        columns = pl.ds(j * width, width)
        if o == 0:
            return stage.at[w, 0, e, :, columns]
        return crossed.at[w, o - 1, e, :, columns]

    def fan(e, w, o):
        begin = lax.rem(tp - o + n_tp, n_tp) * per
        for j in range(per):
            if o:
                over_tp(e, w, o, j).wait_recv()
            to = begin + j
            k = lax.rem(to - fs + n_fs, n_fs)
            target = outs[w].at[e, rows_of(gr, fs)]

            @pl.when(to != fs)
            def _():
                pltpu.make_async_remote_copy(
                    source(e, w, o, j), target, s_send.at[w, e, k], s_recv.at[w, e, k],
                    device_id=(gr, to, tp), device_id_type=MESH,
                ).start()

            @pl.when(to == fs)
            def _():
                pltpu.make_async_copy(source(e, w, o, j), target, own_sem.at[w, e]).start()

    def arrival(e, w, k):
        piece = outs[w].at[e, rows_of(gr, lax.rem(fs - k + n_fs, n_fs))]
        return pltpu.make_async_remote_copy(
            piece, piece, s_send.at[w, e, k], s_recv.at[w, e, k],
            device_id=(gr, lax.rem(fs + k, n_fs), tp), device_id_type=MESH,
        )

    def own_copy(e, w):
        return pltpu.make_async_copy(
            source(e, w, 0, 0), outs[w].at[e, rows_of(gr, fs)], own_sem.at[w, e]
        )

    def over_gr(e, w, k, o, group):
        piece = outs[w].at[e, rows_of(group, lax.rem(fs - k + n_fs, n_fs))]
        return pltpu.make_async_remote_copy(
            piece, piece, d_send.at[w, e, k, o - 1], d_recv.at[w, e, k, o - 1],
            device_id=(lax.rem(gr + o, n_gr), fs, tp), device_id_type=MESH,
        )

    def down_block(group, t):
        return pl.ds(pl.multiple_of((group * n_tp + t) * down_cols, down_cols), down_cols)

    def down_over_tp(e, o):
        return pltpu.make_async_remote_copy(
            stage_down.at[o, e], down_out.at[e, :, down_block(gr, tp)],
            xd_send.at[o - 1, e], xd_recv.at[o - 1, e],
            device_id=(gr, fs, tp_at(o)), device_id_type=MESH,
        )

    def down_arrival(e, o):
        piece = down_out.at[e, :, down_block(gr, lax.rem(tp - o + n_tp, n_tp))]
        return pltpu.make_async_remote_copy(
            piece, piece, xd_send.at[o - 1, e], xd_recv.at[o - 1, e],
            device_id=(gr, fs, tp_at(o)), device_id_type=MESH,
        )

    def down_own(e):
        return pltpu.make_async_copy(
            stage_down.at[0, e], down_out.at[e, :, down_block(gr, tp)], own_down_sem.at[e]
        )

    def down_over_gr(e, s, o, group):
        piece = down_out.at[e, :, down_block(group, lax.rem(tp - s + n_tp, n_tp))]
        return pltpu.make_async_remote_copy(
            piece, piece, dd_send.at[e, s, o - 1], dd_recv.at[e, s, o - 1],
            device_id=(lax.rem(gr + o, n_gr), fs, tp), device_id_type=MESH,
        )

    for w, o in order:
        load(0, w, o).start()
    for o in range(n_tp):
        load_down(0, o).start()
    pl.semaphore_wait(barrier, peers)

    def cast(e):
        for w, o in order:
            load(e, w, o).wait()
            stage[w, o, e] = (raw[w, o] * gain_ref[...]).astype(BF16)

            @pl.when(e + 1 < experts)
            def _():
                load(e + 1, w, o).start()

            if o:
                for j in range(per):
                    over_tp(e, w, o, j).start()
            else:
                fan(e, w, 0)

    def forward(e):
        for w in range(2):
            for o in range(1, n_tp):
                fan(e, w, o)

    cast(0)

    @pl.loop(1, experts)
    def _(e):
        cast(e)
        forward(e - 1)

    @pl.loop(0, experts)
    def _(e):
        for o in [*range(1, n_tp), 0]:
            load_down(e, o).wait()
            stage_down[o, e] = raw_down[o].astype(BF16)

            @pl.when(e + 1 < experts)
            def _():
                load_down(e + 1, o).start()

            if o:
                down_over_tp(e, o).start()
            else:
                down_own(e).start()

    def collect(e):
        for w in range(2):
            own_copy(e, w).wait()
            for o in range(1, n_gr):
                over_gr(e, w, 0, o, gr).start()

        @pl.loop(1, n_fs)
        def _(k):
            for w in range(2):
                arrival(e, w, k).wait_recv()
                for o in range(1, n_gr):
                    over_gr(e, w, k, o, gr).start()

    forward(experts - 1)

    @pl.loop(0, experts - 1)
    def _(e):
        collect(e)

    @pl.loop(0, experts)
    def _(e):
        down_own(e).wait()
        for s in range(1, n_tp):
            down_arrival(e, s).wait_recv()
        for s in range(n_tp):
            for o in range(1, n_gr):
                down_over_gr(e, s, o, gr).start()

    collect(experts - 1)

    @pl.loop(0, experts)
    def _(e):
        for w in range(2):
            for o in range(1, n_tp):
                for j in range(per):
                    over_tp(e, w, o, j).wait_send()

            @pl.loop(1, n_fs)
            def _(k):
                arrival(e, w, k).wait_send()

            @pl.loop(0, n_fs)
            def _(k):
                for o in range(1, n_gr):
                    over_gr(e, w, k, o, gr).wait_send()
                    over_gr(e, w, k, o, lax.rem(gr - o + n_gr, n_gr)).wait_recv()

        for s in range(1, n_tp):
            down_over_tp(e, s).wait_send()
        for s in range(n_tp):
            for o in range(1, n_gr):
                down_over_gr(e, s, o, gr).wait_send()
                down_over_gr(e, s, o, lax.rem(gr - o + n_gr, n_gr)).wait_recv()


def exchange(sizes, norm_gain, gate_master, up_master, down_master):
    n_gr, n_fs, n_tp = sizes
    all_experts, rows, cols = gate_master.shape
    experts = all_experts // n_tp
    width = cols * n_tp // n_fs
    hidden, down_cols = down_master.shape[1], down_master.shape[2]
    any_spec = pl.BlockSpec(memory_space=pl.ANY)
    dma = pltpu.SemaphoreType.DMA
    up_shape = jax.ShapeDtypeStruct((experts, rows * n_gr * n_fs, width), BF16)
    return pl.pallas_call(
        functools.partial(exchange_kernel, n_gr, n_fs, n_tp),
        out_shape=(
            up_shape,
            up_shape,
            jax.ShapeDtypeStruct((experts, hidden, down_cols * n_gr * n_tp), BF16),
        ),
        in_specs=[pl.BlockSpec(memory_space=pltpu.VMEM), any_spec, any_spec, any_spec],
        out_specs=(any_spec, any_spec, any_spec),
        scratch_shapes=[
            pltpu.VMEM((2, n_tp, experts, rows, cols), BF16),
            pltpu.VMEM((n_tp, experts, hidden, down_cols), BF16),
            pltpu.VMEM((2, n_tp - 1, experts, rows, cols), BF16),
            pltpu.VMEM((2, n_tp, rows, cols), jnp.float32),
            pltpu.VMEM((n_tp, hidden, down_cols), jnp.float32),
            dma((2, n_tp)),
            dma((n_tp,)),
            dma((2, n_tp - 1, experts, n_fs // n_tp)),
            dma((2, n_tp - 1, experts, n_fs // n_tp)),
            dma((2, experts, n_fs)),
            dma((2, experts, n_fs)),
            dma((2, experts)),
            dma((2, experts, n_fs, n_gr - 1)),
            dma((2, experts, n_fs, n_gr - 1)),
            dma((n_tp - 1, experts)),
            dma((n_tp - 1, experts)),
            dma((experts,)),
            dma((experts, n_tp, n_gr - 1)),
            dma((experts, n_tp, n_gr - 1)),
        ],
        compiler_params=pltpu.CompilerParams(
            collective_id=0, has_side_effects=True, vmem_limit_bytes=52 * 1024 * 1024
        ),
        cost_estimate=pl.CostEstimate(flops=0, bytes_accessed=1_000_000_000, transcendentals=0),
    )(norm_gain[:, None], gate_master, up_master, down_master)


def experts_kernel(pieces, gate_in, up_in, down_in, gate_out, up_out, down_out, partial, gate_act, up_act, hidden):
    depth = 256
    gate_act[...] = jnp.zeros_like(gate_act)
    up_act[...] = jnp.zeros_like(up_act)

    @pl.loop(0, gate_in.shape[1] // depth)
    def _(i):
        span = pl.ds(pl.multiple_of(i * depth, depth), depth)
        x = pieces[0, :, span]
        gate = gate_in[0, span, :]
        gate_out[0, span, :] = gate
        gate_act[...] += jnp.dot(x, gate, preferred_element_type=jnp.float32)
        up = up_in[0, span, :]
        up_out[0, span, :] = up
        up_act[...] += jnp.dot(x, up, preferred_element_type=jnp.float32)

    hidden[...] = (jax.nn.silu(gate_act[...]) * up_act[...]).astype(BF16)

    @pl.loop(0, down_in.shape[2] // depth)
    def _(i):
        span = pl.ds(pl.multiple_of(i * depth, depth), depth)
        down = down_in[0, :, span]
        down_out[0, :, span] = down
        partial[0, :, span] = jnp.dot(
            hidden[...], down, preferred_element_type=jnp.float32
        ).astype(BF16)


def run_experts(pieces, gate, up, down):
    experts, features, width = gate.shape
    count = pieces.shape[1]

    def whole(*shape):
        return pl.BlockSpec((1, *shape), lambda e: (e, 0, 0))

    weights = [whole(features, width), whole(features, width), whole(width, features)]
    return pl.pallas_call(
        experts_kernel,
        grid=(experts,),
        out_shape=(
            jax.ShapeDtypeStruct(gate.shape, BF16),
            jax.ShapeDtypeStruct(up.shape, BF16),
            jax.ShapeDtypeStruct(down.shape, BF16),
            jax.ShapeDtypeStruct(pieces.shape, BF16),
        ),
        in_specs=[whole(count, features), *weights],
        out_specs=(*weights, whole(count, features)),
        scratch_shapes=[
            pltpu.VMEM((count, width), jnp.float32),
            pltpu.VMEM((count, width), jnp.float32),
            pltpu.VMEM((count, width), BF16),
        ],
        compiler_params=pltpu.CompilerParams(vmem_limit_bytes=60 * 1024 * 1024),
    )(pieces, gate, up, down)


def combine_kernel(
    n_fs, n_tp, part, combiner, out,
    near, summed, far, total, block, others,
    y_send, y_recv, z_send, z_recv, t_send, t_recv,
):
    gr, fs, tp = (lax.axis_index(name) for name in ("gr", "fs", "tp"))
    pairs = n_fs // 2
    z, y = fs // 2, lax.rem(fs, 2)
    experts, _, _, cap, features = part.shape

    barrier = pltpu.get_barrier_semaphore()
    pl.semaphore_signal(barrier, 1, device_id=(gr, z * 2 + 1 - y, tp), device_id_type=MESH)
    for k in range(1, pairs):
        pl.semaphore_signal(
            barrier, 1, device_id=(gr, lax.rem(z + k, pairs) * 2 + y, tp), device_id_type=MESH
        )
    for o in range(1, n_tp):
        pl.semaphore_signal(barrier, 1, device_id=(gr, fs, lax.rem(tp + o, n_tp)), device_id_type=MESH)
    pl.semaphore_wait(barrier, pairs + n_tp - 1)

    def over_pair(e):
        return pltpu.make_async_remote_copy(
            part.at[e, :, 1 - y], near.at[e], y_send.at[e], y_recv.at[e],
            device_id=(gr, z * 2 + 1 - y, tp), device_id_type=MESH,
        )

    def over_pairs(e, k):
        to = lax.rem(z + k, pairs)
        return pltpu.make_async_remote_copy(
            summed.at[e, to], far.at[k - 1, e], z_send.at[k - 1, e], z_recv.at[k - 1, e],
            device_id=(gr, to * 2 + y, tp), device_id_type=MESH,
        )

    def over_tp(o):
        return pltpu.make_async_remote_copy(
            block, others.at[o - 1], t_send.at[o - 1], t_recv.at[o - 1],
            device_id=(gr, fs, lax.rem(tp + o, n_tp)), device_id_type=MESH,
        )

    @pl.loop(0, experts)
    def _(e):
        over_pair(e).start()

    @pl.loop(0, experts)
    def _(e):
        over_pair(e).wait_recv()
        summed[e] = (part[e, :, y].astype(jnp.float32) + near[e].astype(jnp.float32)).astype(BF16)
        for k in range(1, pairs):
            over_pairs(e, k).start()

    @pl.loop(0, experts)
    def _(e):
        value = summed[e, z].astype(jnp.float32)
        for k in range(1, pairs):
            over_pairs(e, k).wait_recv()
            value = value + far[k - 1, e].astype(jnp.float32)
        total[pl.ds(pl.multiple_of(e * cap, cap), cap), :] = value

    tile = 512

    @pl.loop(0, features // tile)
    def _(i):
        span = pl.ds(pl.multiple_of(i * tile, tile), tile)
        block[:, span] = jnp.dot(
            combiner[...], total[:, span], preferred_element_type=jnp.float32,
            precision=lax.Precision.HIGHEST,
        ).astype(BF16)

    for o in range(1, n_tp):
        over_tp(o).start()
    mixed = block[...].astype(jnp.float32)
    for o in range(1, n_tp):
        over_tp(o).wait_recv()
        mixed = mixed + others[o - 1].astype(jnp.float32)
    out[...] = mixed.astype(BF16)

    @pl.loop(0, experts)
    def _(e):
        over_pair(e).wait_send()
        for k in range(1, pairs):
            over_pairs(e, k).wait_send()

    for o in range(1, n_tp):
        over_tp(o).wait_send()


def combine(n_fs, n_tp, partial, combiner):
    experts, count, features = partial.shape
    pairs, cap, tokens = n_fs // 2, count // n_fs, combiner.shape[0]
    dma = pltpu.SemaphoreType.DMA
    vmem = pl.BlockSpec(memory_space=pltpu.VMEM)
    return pl.pallas_call(
        functools.partial(combine_kernel, n_fs, n_tp),
        out_shape=jax.ShapeDtypeStruct((tokens, features), BF16),
        in_specs=[vmem, vmem],
        out_specs=vmem,
        scratch_shapes=[
            pltpu.VMEM((experts, pairs, cap, features), BF16),
            pltpu.VMEM((experts, pairs, cap, features), BF16),
            pltpu.VMEM((pairs - 1, experts, cap, features), BF16),
            pltpu.VMEM((experts * cap, features), jnp.float32),
            pltpu.VMEM((tokens, features), BF16),
            pltpu.VMEM((n_tp - 1, tokens, features), BF16),
            dma((experts,)),
            dma((experts,)),
            dma((pairs - 1, experts)),
            dma((pairs - 1, experts)),
            dma((n_tp - 1,)),
            dma((n_tp - 1,)),
        ],
        compiler_params=pltpu.CompilerParams(
            collective_id=1, has_side_effects=True, vmem_limit_bytes=40 * 1024 * 1024
        ),
    )(partial.reshape(experts, pairs, 2, cap, features), combiner)


def plain_local(tokens, route_ids, route_logits, norm_gain, gate_master, up_master, down_master):
    gain_rows = norm_gain[None, :, None]
    gate_half = (gate_master * gain_rows).astype(jnp.bfloat16)
    up_half = (up_master * gain_rows).astype(jnp.bfloat16)
    down_half = down_master.astype(jnp.bfloat16)
    gate_cols, up_cols, down_cols = (
        lax.all_to_all(gate_half, "tp", split_axis=0, concat_axis=2, tiled=True),
        lax.all_to_all(up_half, "tp", split_axis=0, concat_axis=2, tiled=True),
        lax.all_to_all(down_half, "tp", split_axis=0, concat_axis=2, tiled=True),
    )
    gate_part, up_part = (
        lax.all_to_all(gate_cols, "fs", split_axis=2, concat_axis=1, tiled=True),
        lax.all_to_all(up_cols, "fs", split_axis=2, concat_axis=1, tiled=True),
    )
    gate_weight, up_weight, down_weight = (
        lax.all_gather(gate_part, "gr", axis=1, tiled=True),
        lax.all_gather(up_part, "gr", axis=1, tiled=True),
        lax.all_gather(down_cols, "gr", axis=2, tiled=True),
    )
    as_float = tokens.astype(jnp.float32)
    normed = (
        as_float * lax.rsqrt(jnp.mean(as_float * as_float, axis=-1, keepdims=True) + epsilon)
    ).astype(jnp.bfloat16)
    differ = route_logits[:, 0] - route_logits[:, 1]
    route_weight = jnp.stack([jax.nn.sigmoid(differ), jax.nn.sigmoid(-differ)], axis=1)
    experts_here = gate_weight.shape[0]
    first_expert = lax.axis_index("tp") * experts_here
    expert_ids = first_expert + jnp.arange(experts_here, dtype=jnp.int32)
    route_hits = route_ids[None, :, :] == expert_ids[:, None, None]
    chosen = jnp.any(route_hits, axis=2)
    weight_rows = jnp.sum(jnp.where(route_hits, route_weight[None, :, :], 0.0), axis=2)
    slot_rank = jnp.cumsum(chosen.astype(jnp.int32), axis=1) - 1
    slot_ids = jnp.arange(CAP, dtype=jnp.int32)
    picker = chosen[:, None, :] & (slot_rank[:, None, :] == slot_ids[None, :, None])
    picker_float = picker.astype(jnp.float32)
    packed = jnp.einsum(
        "xsr,rd->sxd", picker.astype(jnp.bfloat16), normed, preferred_element_type=jnp.float32
    ).astype(jnp.bfloat16)
    slot_weight = jnp.einsum(
        "xsr,xr->sx", picker_float, weight_rows, precision=lax.Precision.HIGHEST
    )
    pieces = lax.all_gather(packed, "fs", axis=0, tiled=True)
    gate_act = jnp.einsum("kxd,xdh->kxh", pieces, gate_weight, preferred_element_type=jnp.float32)
    up_act = jnp.einsum("kxd,xdh->kxh", pieces, up_weight, preferred_element_type=jnp.float32)
    hidden = (jax.nn.silu(gate_act) * up_act).astype(jnp.bfloat16)
    expert_out = lax.psum_scatter(
        jnp.einsum("kxh,xhd->kxd", hidden, down_weight, preferred_element_type=jnp.float32).astype(
            jnp.bfloat16
        ),
        "fs",
        scatter_dimension=0,
        tiled=True,
    ).astype(jnp.float32)
    weighted = expert_out * slot_weight[:, :, None]
    block_sum = jnp.einsum("xsr,sxd->rd", picker_float, weighted, precision=lax.Precision.HIGHEST)
    mixed = lax.psum(block_sum.astype(jnp.bfloat16), "tp")
    return (gate_weight, up_weight, down_weight, mixed)


def fast_local(sizes, tokens, route_ids, route_logits, norm_gain, gate_master, up_master, down_master):
    n_gr, n_fs, n_tp = sizes
    gate_moved, up_moved, down_moved = exchange(
        sizes, norm_gain, gate_master, up_master, down_master
    )
    as_float = tokens.astype(jnp.float32)
    normed = (
        as_float * lax.rsqrt(jnp.mean(as_float * as_float, axis=-1, keepdims=True) + epsilon)
    ).astype(jnp.bfloat16)
    differ = route_logits[:, 0] - route_logits[:, 1]
    route_weight = jnp.stack([jax.nn.sigmoid(differ), jax.nn.sigmoid(-differ)], axis=1)
    experts_here = gate_moved.shape[0]
    first_expert = lax.axis_index("tp") * experts_here
    expert_ids = first_expert + jnp.arange(experts_here, dtype=jnp.int32)
    route_hits = route_ids[None, :, :] == expert_ids[:, None, None]
    chosen = jnp.any(route_hits, axis=2)
    weight_rows = jnp.sum(jnp.where(route_hits, route_weight[None, :, :], 0.0), axis=2)
    slot_rank = jnp.cumsum(chosen.astype(jnp.int32), axis=1) - 1
    slot_ids = jnp.arange(CAP, dtype=jnp.int32)
    picker = chosen[:, None, :] & (slot_rank[:, None, :] == slot_ids[None, :, None])
    picker_float = picker.astype(jnp.float32)
    packed = jnp.einsum(
        "xsr,rd->xsd", picker.astype(jnp.bfloat16), normed, preferred_element_type=jnp.float32
    ).astype(jnp.bfloat16)
    combiner = jnp.transpose(picker_float * weight_rows[:, None, :], (2, 0, 1))
    pieces = lax.all_gather(packed, "fs", axis=1, tiled=True)
    gate_weight, up_weight, down_weight, partial = run_experts(
        pieces, gate_moved, up_moved, down_moved
    )
    mixed = combine(n_fs, n_tp, partial, combiner.reshape(combiner.shape[0], -1))
    return (gate_weight, up_weight, down_weight, mixed)


def solution(mesh):
    n_gr, n_fs, n_tp = (mesh.shape[name] for name in ("gr", "fs", "tp"))
    placed = (
        P(("gr", "fs"), None),
        P(("gr", "fs"), None),
        P(("gr", "fs"), None),
        P(("gr", "fs")),
        P(None, ("gr", "fs"), "tp"),
        P(None, ("gr", "fs"), "tp"),
        P(None, "fs", ("gr", "tp")),
    )

    def local(tokens, route_ids, route_logits, norm_gain, gate_master, up_master, down_master):
        width = gate_master.shape[2] * n_tp // n_fs
        aligned = width % 128 == 0 and down_master.shape[2] % 128 == 0
        fits = n_fs % n_tp == 0 and n_fs % 2 == 0 and min(n_gr, n_tp) > 1
        run = functools.partial(fast_local, (n_gr, n_fs, n_tp)) if aligned and fits else plain_local
        return run(tokens, route_ids, route_logits, norm_gain, gate_master, up_master, down_master)

    return jax.shard_map(
        local,
        mesh=mesh,
        in_specs=placed,
        out_specs=(
            P("tp", None, "fs"),
            P("tp", None, "fs"),
            P("tp", "fs", None),
            P(("gr", "fs"), None),
        ),
        check_vma=False,
    )
```

profile of v0, /device:TPU:0, one launch (start us, length us, event | category | flops | bytes accessed | tf_op | source)
XLA Modules:
  0.0 527.7 jit_solution(17887198044154250588)
XLA Ops:
  7.2 0.0 all-gather.2.cloned.1.call-start
  7.2 0.8 compare_reduce_fusion
  8.0 0.3 reduce_window_sum.11
  8.3 1.2 fusion
  9.5 2.2 convolution_convert_fusion
  11.8 0.0 all-gather.2.cloned.1.call-update
  11.8 0.8 copy.22.gain_ref
  12.6 0.1 copy.23
  12.7 0.8 add_divide_fusion.1
  13.4 0.8 fusion.9
  14.2 0.1 copy.25
  14.3 0.1 copy.24
  14.5 0.1 eq.49
  14.5 369.2 %shard_map.102 = (bf16[4,2048,896]{2,1,0:T(8,128)(2,1)}, bf16[4,2048,896]{2,1,0:T(8,128)(2,1)}, bf16[4,896,2048]{2,1,0:T(8,128)(2,1)}) custom-call(f32[128,1]{1,0:T(8,128)S(1)} %copy.22.gain_ref, f32[8,128,3584]{2,1,0:T(8,128)} %gate_ref.1, f32[8,128,3584]{2,1,0:T(8,128)} %up_ref.1, f32[8,896,512]{2,1,0:T(8,128)} %down_ref.1), custom_call_target="tpu_custom_call" | custom-call | bytes 1000000000 | tf_op jit(solution)/shard_map/pallas_call | solution.py:257
  383.8 0.0 all-gather.2.cloned.1.call-done.pieces
  383.8 40.5 %shard_map.103 = (bf16[4,2048,896]{2,1,0:T(8,128)(2,1)}, bf16[4,2048,896]{2,1,0:T(8,128)(2,1)}, bf16[4,896,2048]{2,1,0:T(8,128)(2,1)}, bf16[4,256,2048]{2,1,0:T(8,128)(2,1)}) custom-call(bf16[4,256,2048]{2,1,0:T(8,128)(2,1)} %all-gather.2.cloned.1.call-done.pieces, bf16[4,2048,896]{2,1,0:T(8,128)(2,1)} %get-tuple-element.11.gate_in, ...), custom_call_target="tpu_custom_call" | custom-call | tf_op jit(solution)/shard_map/pallas_call | solution.py:330
  424.3 0.0 copy-start
  424.3 2.2 copy-done
  426.5 93.6 %shard_map.104 = bf16[128,2048]{1,0:T(8,128)(2,1)S(1)} custom-call(bf16[4,4,2,32,2048]{4,3,2,1,0:T(8,128)(2,1)S(1)} %bitcast.12, f32[128,128]{1,0:T(8,128)S(1)} %and_select_fusion.combiner), custom_call_target="tpu_custom_call" | custom-call | tf_op jit(solution)/shard_map/pallas_call | solution.py:441
  520.1 0.8 copy.27
  (10 shorter events, 0.1 us)
Async XLA Ops:
  7.2 376.6 %all-gather.2.cloned.1.call-start = ((), (), s32[]{:S(2)}) async-start(), calls=%async_computation | async-start | bytes 4718592 | tf_op jit(solution)/shard_map/all_gather | solution.py:550
  424.3 2.2 copy-start
Sparse Core Ops, SparseCore 0:
  11.9 216.0 all-gather.1
where the time goes:
time: 528 us
  Pallas kernels  503 us (95%)
  between operations  14.1 us (3%)
    pallas_call x1, Pallas kernels, exchange(): pl.pallas_call(functools.partial(exchange_kernel, n_gr, n_fs, n_tp), out_...  369 us
    pallas_call x1, Pallas kernels, combine(): pl.pallas_call(functools.partial(combine_kernel, n_fs, n_tp), out_shape=j...  93.6 us
    pallas_call x1, Pallas kernels, run_experts(): pl.pallas_call(experts_kernel, grid=(experts,), out_shape=(jax.ShapeDtype...  40.5 us
  transfers between devices with their start and end apart: 1, of which 0 were waited for; matrix products, arithmetic and copies ran while one was open for 1% of the time, Pallas kernels for 70%

commit v1 on v0

--- a/solution.py
+++ b/solution.py
@@ -17,11 +17,12 @@
 
 def exchange_kernel(
     n_gr, n_fs, n_tp,
-    gain_ref, gate_ref, up_ref, down_ref,
-    gate_out, up_out, down_out,
+    gain_ref, gate_ref, up_ref, down_ref, packed_ref,
+    gate_out, up_out, down_out, pieces,
     stage, stage_down, crossed, raw, raw_down,
     load_sem, load_down_sem, x_send, x_recv, s_send, s_recv, own_sem,
     d_send, d_recv, xd_send, xd_recv, own_down_sem, dd_send, dd_recv,
+    p_send, p_recv, p_own,
 ):
     gr, fs, tp = (lax.axis_index(name) for name in ("gr", "fs", "tp"))
     experts, _, width = gate_out.shape
@@ -142,11 +143,64 @@
             device_id=(lax.rem(gr + o, n_gr), fs, tp), device_id_type=MESH,
         )
 
+    pairs = n_fs // 2
+    z, y = fs // 2, lax.rem(fs, 2)
+
+    def relay(kind, hop):
+        at = {"up": z - hop, "down": z + hop, "over": z - hop, "over_down": z + hop}[kind]
+        to = {"up": fs + 2, "down": fs - 2}.get(kind, fs + 1 - 2 * y)
+        origin = at * 2 + y
+        here = packed_ref if hop == 0 else pieces.at[:, origin]
+        slot = ["up", "down", "over", "over_down"].index(kind)
+        return pltpu.make_async_remote_copy(
+            here, pieces.at[:, origin], p_send.at[slot, hop], p_recv.at[origin],
+            device_id=(gr, to, tp), device_id_type=MESH,
+        )
+
+    def landed(origin):
+        piece = pieces.at[:, origin]
+        return pltpu.make_async_remote_copy(
+            piece, piece, p_send.at[0, 0], p_recv.at[origin],
+            device_id=(gr, fs + 1 - 2 * y, tp), device_id_type=MESH,
+        )
+
+    def relayed(kind, hop):
+        if kind == "up":
+            return (z - hop >= 0) & (z + 1 < pairs)
+        if kind == "down":
+            return (z + hop < pairs) & (z >= 1)
+        return z - hop >= 0 if kind == "over" else z + hop < pairs
+
+    def relay_start(kind, hop):
+        @pl.when(relayed(kind, hop))
+        def _():
+            relay(kind, hop).start()
+
+    def relay_from(hop):
+        @pl.when(z - hop >= 0)
+        def _():
+            landed((z - hop) * 2 + y).wait_recv()
+            relay(kind="over", hop=hop).start()
+
+        relay_start("up", hop)
+
+        @pl.when(z + hop < pairs)
+        def _():
+            landed((z + hop) * 2 + y).wait_recv()
+            relay(kind="over_down", hop=hop).start()
+
+        relay_start("down", hop)
+
+    own_piece = pltpu.make_async_copy(packed_ref, pieces.at[:, fs], p_own)
+
     for w, o in order:
         load(0, w, o).start()
     for o in range(n_tp):
         load_down(0, o).start()
     pl.semaphore_wait(barrier, peers)
+    for kind in ("up", "down", "over"):
+        relay_start(kind, 0)
+    own_piece.start()
 
     def cast(e):
         for w, o in order:
@@ -174,6 +228,9 @@
     def _(e):
         cast(e)
         forward(e - 1)
+
+    for hop in range(1, pairs):
+        relay_from(hop)
 
     @pl.loop(0, experts)
     def _(e):
@@ -244,8 +301,17 @@
                 down_over_gr(e, s, o, gr).wait_send()
                 down_over_gr(e, s, o, lax.rem(gr - o + n_gr, n_gr)).wait_recv()
 
-
-def exchange(sizes, norm_gain, gate_master, up_master, down_master):
+    own_piece.wait()
+    for at in range(pairs):
+        landed(at * 2 + 1 - y).wait_recv()
+    for kind in ("up", "down", "over", "over_down"):
+        for hop in range(1 if kind == "over_down" else 0, pairs):
+            @pl.when(relayed(kind, hop))
+            def _():
+                relay(kind, hop).wait_send()
+
+
+def exchange(sizes, norm_gain, gate_master, up_master, down_master, packed):
     n_gr, n_fs, n_tp = sizes
     all_experts, rows, cols = gate_master.shape
     experts = all_experts // n_tp
@@ -260,9 +326,10 @@
             up_shape,
             up_shape,
             jax.ShapeDtypeStruct((experts, hidden, down_cols * n_gr * n_tp), BF16),
+            jax.ShapeDtypeStruct((packed.shape[0], n_fs, *packed.shape[1:]), BF16),
         ),
-        in_specs=[pl.BlockSpec(memory_space=pltpu.VMEM), any_spec, any_spec, any_spec],
-        out_specs=(any_spec, any_spec, any_spec),
+        in_specs=[pl.BlockSpec(memory_space=pltpu.VMEM), *[any_spec] * 4],
+        out_specs=(any_spec,) * 4,
         scratch_shapes=[
             pltpu.VMEM((2, n_tp, experts, rows, cols), BF16),
             pltpu.VMEM((n_tp, experts, hidden, down_cols), BF16),
@@ -283,184 +350,273 @@
             dma((experts,)),
             dma((experts, n_tp, n_gr - 1)),
             dma((experts, n_tp, n_gr - 1)),
+            dma((4, n_fs // 2)),
+            dma((n_fs,)),
+            dma,
         ],
         compiler_params=pltpu.CompilerParams(
             collective_id=0, has_side_effects=True, vmem_limit_bytes=52 * 1024 * 1024
         ),
         cost_estimate=pl.CostEstimate(flops=0, bytes_accessed=1_000_000_000, transcendentals=0),
-    )(norm_gain[:, None], gate_master, up_master, down_master)
-
-
-def experts_kernel(pieces, gate_in, up_in, down_in, gate_out, up_out, down_out, partial, gate_act, up_act, hidden):
-    depth = 256
-    gate_act[...] = jnp.zeros_like(gate_act)
-    up_act[...] = jnp.zeros_like(up_act)
-
-    @pl.loop(0, gate_in.shape[1] // depth)
-    def _(i):
-        span = pl.ds(pl.multiple_of(i * depth, depth), depth)
-        x = pieces[0, :, span]
-        gate = gate_in[0, span, :]
-        gate_out[0, span, :] = gate
-        gate_act[...] += jnp.dot(x, gate, preferred_element_type=jnp.float32)
-        up = up_in[0, span, :]
-        up_out[0, span, :] = up
-        up_act[...] += jnp.dot(x, up, preferred_element_type=jnp.float32)
-
-    hidden[...] = (jax.nn.silu(gate_act[...]) * up_act[...]).astype(BF16)
-
-    @pl.loop(0, down_in.shape[2] // depth)
-    def _(i):
-        span = pl.ds(pl.multiple_of(i * depth, depth), depth)
-        down = down_in[0, :, span]
-        down_out[0, :, span] = down
-        partial[0, :, span] = jnp.dot(
-            hidden[...], down, preferred_element_type=jnp.float32
-        ).astype(BF16)
+    )(norm_gain[:, None], gate_master, up_master, down_master, packed)
+
+
+def experts_kernel(
+    slices, lead,
+    pieces, gate_in, up_in, down_in,
+    gate_out, up_out, down_out, sums,
+    tall, wide, partial, gate_act, up_act, hidden,
+    tall_load, tall_store, wide_load, wide_store,
+):
+    experts, features, width = gate_in.shape
+    depth, cols = tall.shape[1], wide.shape[2]
+    steps, ring = 2 * slices, tall.shape[0]
+    count = hidden.shape[1]
+    owners, tokens = sums.shape[0], sums.shape[1]
+    ins, outs = (gate_in, up_in), (gate_out, up_out)
+
+    def tall_ends(refs, e, j):
+        return refs[j % 2].at[e, pl.ds(j // 2 * depth, depth)]
+
+    def tall_slot(e, j):
+        return lax.rem(e * steps + j, ring)
+
+    def load_tall(e, j):
+        slot = tall_slot(e, j)
+        return pltpu.make_async_copy(tall_ends(ins, e, j), tall.at[slot], tall_load.at[slot])
+
+    def store_tall(e, j):
+        slot = tall_slot(e, j)
+        return pltpu.make_async_copy(tall.at[slot], tall_ends(outs, e, j), tall_store.at[slot])
+
+    def span(c):
+        return pl.ds(pl.multiple_of(c * cols, cols), cols)
+
+    def load_wide(c, e):
+        slot = c * experts + e
+        return pltpu.make_async_copy(down_in.at[e, :, span(c)], wide.at[slot], wide_load.at[slot])
+
+    def store_wide(c, e):
+        slot = c * experts + e
+        return pltpu.make_async_copy(wide.at[slot], down_out.at[e, :, span(c)], wide_store.at[slot])
+
+    for j in range(lead):
+        load_tall(j // steps, j % steps).start()
+
+    @pl.loop(0, experts)
+    def _(e):
+        for j in range(steps):
+            load_tall(e, j).wait()
+            store_tall(e, j).start()
+            later, k = e + (j + lead) // steps, (j + lead) % steps
+
+            @pl.when(later < experts)
+            def _():
+                @pl.when(later * steps + k >= ring)
+                def _():
+                    before = later * steps + k - ring
+                    store_tall(before // steps, k).wait()
+
+                load_tall(later, k).start()
+
+            @pl.when(e == experts - 1)
+            def _():
+                for i in range(j, slices * experts // 2, steps):
+                    load_wide(i // experts, i % experts).start()
+
+            act = (gate_act, up_act)[j % 2]
+            x = pieces[e, :, :, pl.ds(j // 2 * depth, depth)].reshape(count, depth)
+            value = jnp.dot(x, tall[tall_slot(e, j)], preferred_element_type=jnp.float32)
+            if j < 2:
+                act[...] = value
+            else:
+                act[...] += value
+        hidden[e] = (jax.nn.silu(gate_act[...]) * up_act[...]).astype(BF16)
+
+    half = slices * experts // 2
+
+    @pl.loop(0, slices)
+    def _(c):
+        for e in range(experts):
+            load_wide(c, e).wait()
+            store_wide(c, e).start()
+            ahead = c * experts + e + half
+
+            @pl.when(ahead < slices * experts)
+            def _():
+                load_wide(ahead // experts, lax.rem(ahead, experts)).start()
+
+            value = jnp.dot(hidden[e], wide[c * experts + e], preferred_element_type=jnp.float32)
+            partial[e] = value.astype(BF16).reshape(partial.shape[1:])
+
+        for o in range(owners):
+            weights = pieces[:, o, :, pl.ds(features, tokens)].reshape(-1, tokens)
+            rows = partial[:, o].reshape(-1, cols)
+            sums[o, :, span(c)] = lax.dot_general(
+                weights, rows, (((0,), (0,)), ((), ())), preferred_element_type=jnp.float32
+            ).astype(BF16)
+
+    for i in range(ring):
+        at = experts * steps - ring + i
+        store_tall(at // steps, at % steps).wait()
+    for c in range(slices):
+        for e in range(experts):
+            store_wide(c, e).wait()
 
 
 def run_experts(pieces, gate, up, down):
     experts, features, width = gate.shape
-    count = pieces.shape[1]
-
-    def whole(*shape):
-        return pl.BlockSpec((1, *shape), lambda e: (e, 0, 0))
-
-    weights = [whole(features, width), whole(features, width), whole(width, features)]
+    _, owners, cap, padded = pieces.shape
+    tokens, count, slices = padded - features, owners * cap, 4
+    ring = 2 * 2 * slices
+    any_spec = pl.BlockSpec(memory_space=pl.ANY)
+    vmem = pl.BlockSpec(memory_space=pltpu.VMEM)
+    dma = pltpu.SemaphoreType.DMA
     return pl.pallas_call(
-        experts_kernel,
-        grid=(experts,),
+        functools.partial(experts_kernel, slices, 2 * slices),
         out_shape=(
             jax.ShapeDtypeStruct(gate.shape, BF16),
             jax.ShapeDtypeStruct(up.shape, BF16),
             jax.ShapeDtypeStruct(down.shape, BF16),
-            jax.ShapeDtypeStruct(pieces.shape, BF16),
+            jax.ShapeDtypeStruct((owners, tokens, features), BF16),
         ),
-        in_specs=[whole(count, features), *weights],
-        out_specs=(*weights, whole(count, features)),
+        in_specs=[vmem, any_spec, any_spec, any_spec],
+        out_specs=(any_spec, any_spec, any_spec, vmem),
         scratch_shapes=[
+            pltpu.VMEM((ring, features // slices, width), BF16),
+            pltpu.VMEM((slices * experts, width, features // slices), BF16),
+            pltpu.VMEM((experts, owners, cap, features // slices), BF16),
             pltpu.VMEM((count, width), jnp.float32),
             pltpu.VMEM((count, width), jnp.float32),
-            pltpu.VMEM((count, width), BF16),
+            pltpu.VMEM((experts, count, width), BF16),
+            dma((ring,)),
+            dma((ring,)),
+            dma((slices * experts,)),
+            dma((slices * experts,)),
         ],
-        compiler_params=pltpu.CompilerParams(vmem_limit_bytes=60 * 1024 * 1024),
+        compiler_params=pltpu.CompilerParams(vmem_limit_bytes=44 * 1024 * 1024),
+        cost_estimate=pl.CostEstimate(
+            flops=6 * experts * count * features * width,
+            bytes_accessed=12 * experts * features * width, transcendentals=0,
+        ),
     )(pieces, gate, up, down)
 
 
-def combine_kernel(
-    n_fs, n_tp, part, combiner, out,
-    near, summed, far, total, block, others,
-    y_send, y_recv, z_send, z_recv, t_send, t_recv,
-):
+def plan_of(n_bits, features):
+    rest = list(range(2, n_bits))
+    orders = ([0, "x", 1, *rest], ["x", 1, 0, *rest], [1, 0, "x", *rest])
+    unit = 128
+    units = features // unit
+    shares, chunks, begin = [], [], 0
+    for i in range(6):
+        shares.append((units - sum(shares)) // (6 - i))
+    for i, share in enumerate(shares):
+        if share:
+            chunks.append((orders[i % 3], begin * unit, share * unit))
+        begin += share
+    return chunks
+
+
+def combine_kernel(n_fs, chunks, sums, out, acc, *rest):
+    stages = len(chunks[0][0])
+    boxes, (s_send, s_recv, o_send, o_recv) = rest[:-4], rest[-4:]
     gr, fs, tp = (lax.axis_index(name) for name in ("gr", "fs", "tp"))
-    pairs = n_fs // 2
-    z, y = fs // 2, lax.rem(fs, 2)
-    experts, _, _, cap, features = part.shape
+    n_bits = stages - 1
+    rows = sums.shape[-2]
+    bits = [lax.rem(fs // (1 << b), 2) for b in range(n_bits)]
+
+    def mine(dim):
+        return tp if dim == "x" else bits[dim]
+
+    def partner(dim):
+        if dim == "x":
+            return (gr, fs, 1 - tp)
+        return (gr, fs + (1 - 2 * bits[dim]) * (1 << dim), tp)
+
+    def block(order, stage, own, cols):
+        index = [slice(None)] * (n_bits + 1)
+        for dim in order[: stage + 1]:
+            at = n_bits if dim == "x" else n_bits - 1 - dim
+            index[at] = mine(dim)
+            if dim == order[stage] and not own:
+                index[at] = 1 - mine(dim)
+        return (*index, slice(None), cols)
 
     barrier = pltpu.get_barrier_semaphore()
-    pl.semaphore_signal(barrier, 1, device_id=(gr, z * 2 + 1 - y, tp), device_id_type=MESH)
-    for k in range(1, pairs):
-        pl.semaphore_signal(
-            barrier, 1, device_id=(gr, lax.rem(z + k, pairs) * 2 + y, tp), device_id_type=MESH
-        )
-    for o in range(1, n_tp):
-        pl.semaphore_signal(barrier, 1, device_id=(gr, fs, lax.rem(tp + o, n_tp)), device_id_type=MESH)
-    pl.semaphore_wait(barrier, pairs + n_tp - 1)
-
-    def over_pair(e):
-        return pltpu.make_async_remote_copy(
-            part.at[e, :, 1 - y], near.at[e], y_send.at[e], y_recv.at[e],
-            device_id=(gr, z * 2 + 1 - y, tp), device_id_type=MESH,
-        )
-
-    def over_pairs(e, k):
-        to = lax.rem(z + k, pairs)
-        return pltpu.make_async_remote_copy(
-            summed.at[e, to], far.at[k - 1, e], z_send.at[k - 1, e], z_recv.at[k - 1, e],
-            device_id=(gr, to * 2 + y, tp), device_id_type=MESH,
-        )
-
-    def over_tp(o):
-        return pltpu.make_async_remote_copy(
-            block, others.at[o - 1], t_send.at[o - 1], t_recv.at[o - 1],
-            device_id=(gr, fs, lax.rem(tp + o, n_tp)), device_id_type=MESH,
-        )
-
-    @pl.loop(0, experts)
-    def _(e):
-        over_pair(e).start()
-
-    @pl.loop(0, experts)
-    def _(e):
-        over_pair(e).wait_recv()
-        summed[e] = (part[e, :, y].astype(jnp.float32) + near[e].astype(jnp.float32)).astype(BF16)
-        for k in range(1, pairs):
-            over_pairs(e, k).start()
-
-    @pl.loop(0, experts)
-    def _(e):
-        value = summed[e, z].astype(jnp.float32)
-        for k in range(1, pairs):
-            over_pairs(e, k).wait_recv()
-            value = value + far[k - 1, e].astype(jnp.float32)
-        total[pl.ds(pl.multiple_of(e * cap, cap), cap), :] = value
-
-    tile = 512
-
-    @pl.loop(0, features // tile)
-    def _(i):
-        span = pl.ds(pl.multiple_of(i * tile, tile), tile)
-        block[:, span] = jnp.dot(
-            combiner[...], total[:, span], preferred_element_type=jnp.float32,
-            precision=lax.Precision.HIGHEST,
-        ).astype(BF16)
-
-    for o in range(1, n_tp):
-        over_tp(o).start()
-    mixed = block[...].astype(jnp.float32)
-    for o in range(1, n_tp):
-        over_tp(o).wait_recv()
-        mixed = mixed + others[o - 1].astype(jnp.float32)
-    out[...] = mixed.astype(BF16)
-
-    @pl.loop(0, experts)
-    def _(e):
-        over_pair(e).wait_send()
-        for k in range(1, pairs):
-            over_pairs(e, k).wait_send()
-
-    for o in range(1, n_tp):
-        over_tp(o).wait_send()
-
-
-def combine(n_fs, n_tp, partial, combiner):
-    experts, count, features = partial.shape
-    pairs, cap, tokens = n_fs // 2, count // n_fs, combiner.shape[0]
+    for dim in [*range(n_bits), "x"]:
+        pl.semaphore_signal(barrier, 1, device_id=partner(dim), device_id_type=MESH)
+    pl.semaphore_wait(barrier, n_bits + 1)
+
+    def step(i, stage):
+        order, begin, size = chunks[i]
+        held = sums if stage == 0 else acc
+        return pltpu.make_async_remote_copy(
+            held.at[block(order, stage, False, pl.ds(begin, size))],
+            boxes[i * stages + stage], s_send.at[i, stage], s_recv.at[i, stage],
+            device_id=partner(order[stage]), device_id_type=MESH,
+        )
+
+    def finished(i):
+        _, begin, size = chunks[i]
+        here = out.at[pl.ds(pl.multiple_of(tp * rows, rows), rows), pl.ds(begin, size)]
+        return pltpu.make_async_remote_copy(
+            here, here, o_send.at[i], o_recv.at[i], device_id=partner("x"), device_id_type=MESH
+        )
+
+    for i in range(len(chunks)):
+        step(i, 0).start()
+    for stage in range(stages):
+        for i, (order, begin, size) in enumerate(chunks):
+            step(i, stage).wait_recv()
+            at = block(order, stage, True, pl.ds(begin, size))
+            held = sums if stage == 0 else acc
+            value = held[at].astype(jnp.float32) + boxes[i * stages + stage][...].astype(jnp.float32)
+            if stage + 1 < stages:
+                acc[at] = value.astype(BF16)
+                step(i, stage + 1).start()
+            else:
+                out[pl.ds(pl.multiple_of(tp * rows, rows), rows), pl.ds(begin, size)] = value.astype(BF16)
+                finished(i).start()
+    for i in range(len(chunks)):
+        _, begin, size = chunks[i]
+        there = out.at[pl.ds(pl.multiple_of((1 - tp) * rows, rows), rows), pl.ds(begin, size)]
+        pltpu.make_async_remote_copy(
+            there, there, o_send.at[i], o_recv.at[i], device_id=partner("x"), device_id_type=MESH
+        ).wait_recv()
+        finished(i).wait_send()
+        for stage in range(stages):
+            step(i, stage).wait_send()
+
+
+def combine(n_fs, sums):
+    owners, tokens, features = sums.shape
+    n_bits = n_fs.bit_length() - 1
+    stages, rows = n_bits + 1, tokens // 2
+    chunks = plan_of(n_bits, features)
     dma = pltpu.SemaphoreType.DMA
     vmem = pl.BlockSpec(memory_space=pltpu.VMEM)
+    boxes = [
+        pltpu.VMEM((*(2,) * (n_bits - stage), rows, size), BF16)
+        for _, _, size in chunks for stage in range(stages)
+    ]
+    view = (*(2,) * (n_bits + 1), rows, features)
     return pl.pallas_call(
-        functools.partial(combine_kernel, n_fs, n_tp),
+        functools.partial(combine_kernel, n_fs, chunks),
         out_shape=jax.ShapeDtypeStruct((tokens, features), BF16),
-        in_specs=[vmem, vmem],
+        in_specs=[vmem],
         out_specs=vmem,
         scratch_shapes=[
-            pltpu.VMEM((experts, pairs, cap, features), BF16),
-            pltpu.VMEM((experts, pairs, cap, features), BF16),
-            pltpu.VMEM((pairs - 1, experts, cap, features), BF16),
-            pltpu.VMEM((experts * cap, features), jnp.float32),
-            pltpu.VMEM((tokens, features), BF16),
-            pltpu.VMEM((n_tp - 1, tokens, features), BF16),
-            dma((experts,)),
-            dma((experts,)),
-            dma((pairs - 1, experts)),
-            dma((pairs - 1, experts)),
-            dma((n_tp - 1,)),
-            dma((n_tp - 1,)),
+            pltpu.VMEM(view, BF16),
+            *boxes,
+            dma((len(chunks), stages)),
+            dma((len(chunks), stages)),
+            dma((len(chunks),)),
+            dma((len(chunks),)),
         ],
         compiler_params=pltpu.CompilerParams(
             collective_id=1, has_side_effects=True, vmem_limit_bytes=40 * 1024 * 1024
         ),
-    )(partial.reshape(experts, pairs, 2, cap, features), combiner)
+    )(sums.reshape(view))
 
 
 def plain_local(tokens, route_ids, route_logits, norm_gain, gate_master, up_master, down_master):
@@ -524,16 +680,13 @@
 
 def fast_local(sizes, tokens, route_ids, route_logits, norm_gain, gate_master, up_master, down_master):
     n_gr, n_fs, n_tp = sizes
-    gate_moved, up_moved, down_moved = exchange(
-        sizes, norm_gain, gate_master, up_master, down_master
-    )
     as_float = tokens.astype(jnp.float32)
     normed = (
         as_float * lax.rsqrt(jnp.mean(as_float * as_float, axis=-1, keepdims=True) + epsilon)
     ).astype(jnp.bfloat16)
     differ = route_logits[:, 0] - route_logits[:, 1]
     route_weight = jnp.stack([jax.nn.sigmoid(differ), jax.nn.sigmoid(-differ)], axis=1)
-    experts_here = gate_moved.shape[0]
+    experts_here = gate_master.shape[0] // n_tp
     first_expert = lax.axis_index("tp") * experts_here
     expert_ids = first_expert + jnp.arange(experts_here, dtype=jnp.int32)
     route_hits = route_ids[None, :, :] == expert_ids[:, None, None]
@@ -542,17 +695,18 @@
     slot_rank = jnp.cumsum(chosen.astype(jnp.int32), axis=1) - 1
     slot_ids = jnp.arange(CAP, dtype=jnp.int32)
     picker = chosen[:, None, :] & (slot_rank[:, None, :] == slot_ids[None, :, None])
-    picker_float = picker.astype(jnp.float32)
     packed = jnp.einsum(
         "xsr,rd->xsd", picker.astype(jnp.bfloat16), normed, preferred_element_type=jnp.float32
     ).astype(jnp.bfloat16)
-    combiner = jnp.transpose(picker_float * weight_rows[:, None, :], (2, 0, 1))
-    pieces = lax.all_gather(packed, "fs", axis=1, tiled=True)
-    gate_weight, up_weight, down_weight, partial = run_experts(
+    combiner = (picker.astype(jnp.float32) * weight_rows[:, None, :]).astype(jnp.bfloat16)
+    gate_moved, up_moved, down_moved, pieces = exchange(
+        sizes, norm_gain, gate_master, up_master, down_master,
+        jnp.concatenate([packed, combiner], axis=2),
+    )
+    gate_weight, up_weight, down_weight, sums = run_experts(
         pieces, gate_moved, up_moved, down_moved
     )
-    mixed = combine(n_fs, n_tp, partial, combiner.reshape(combiner.shape[0], -1))
-    return (gate_weight, up_weight, down_weight, mixed)
+    return (gate_weight, up_weight, down_weight, combine(n_fs, sums))
 
 
 def solution(mesh):
@@ -570,7 +724,8 @@
     def local(tokens, route_ids, route_logits, norm_gain, gate_master, up_master, down_master):
         width = gate_master.shape[2] * n_tp // n_fs
         aligned = width % 128 == 0 and down_master.shape[2] % 128 == 0
-        fits = n_fs % n_tp == 0 and n_fs % 2 == 0 and min(n_gr, n_tp) > 1
+        fits = n_fs % n_tp == 0 and n_fs & (n_fs - 1) == 0 and n_fs > 2
+        fits = fits and n_gr > 1 and n_tp == 2 and tokens.shape[0] % 128 == 0
         run = functools.partial(fast_local, (n_gr, n_fs, n_tp)) if aligned and fits else plain_local
         return run(tokens, route_ids, route_logits, norm_gain, gate_master, up_master, down_master)
 

time: 528 us -> 539 us (1.021)
  Pallas kernels: 503 us -> 529 us
  between operations: 14.1 us -> 0.7 us
    pallas_call x1, Pallas kernels: 369 us -> 441 us  [exchange(): pl.pallas_call(functools.partial(exchange_kernel, n_gr, n_fs, n_tp), out_...]
    pallas_call x2, Pallas kernels: 134 us -> 88.3 us  [the longest x1 59.1 us: combine(): pl.pallas_call(functools.partial(combine_kernel, n_fs, chunks), out_shape...]
  transfers between devices with their start and end apart: 1 -> 0, of which waited for: 0 -> 0; matrix products, arithmetic and copies ran while one was open for 1% -> 0% of each run, Pallas kernels for 70% -> 0%
where the time goes in v1:
time: 539 us
  Pallas kernels  529 us (98%)
    pallas_call x1, Pallas kernels, exchange(): pl.pallas_call(functools.partial(exchange_kernel, n_gr, n_fs, n_tp), out_...  441 us
    pallas_call x1, Pallas kernels, combine(): pl.pallas_call(functools.partial(combine_kernel, n_fs, chunks), out_shape...  59.1 us
    pallas_call x1, Pallas kernels, run_experts(): pl.pallas_call(functools.partial(experts_kernel, slices, 2 * slices), out...  29.2 us

profile of v1, /device:TPU:0, one launch (start us, length us, event | category | flops | bytes accessed | tf_op | source)
XLA Modules:
  0.0 538.8 jit_solution(4092225004526438062)
XLA Ops:
  0.6 0.8 compare_reduce_fusion
  1.4 1.2 fusion
  2.6 0.8 add_divide_fusion.1
  3.4 0.8 fusion.9
  4.2 0.3 reduce_window_sum.11
  4.5 0.8 copy.14.gain_ref
  5.3 1.4 convolution_convert_fusion
  6.8 440.7 %shard_map.102 = (bf16[4,2048,896]{2,1,0:T(8,128)(2,1)}, bf16[4,2048,896]{2,1,0:T(8,128)(2,1)}, bf16[4,896,2048]{2,1,0:T(8,128)(2,1)}, bf16[4,8,32,2176]{3,2,1,0:T(8,128)(2,1)}) custom-call(f32[128,1]{1,0:T(8,128)S(1)} %copy.14.gain_ref, f32[8,128,3584]{2,1,0:T(8,128)} %gate_ref.1, f32[8,128,3584]{2,1,0:T(8,128)} %up_ref.1, f32[8,896,512]{2,1,0:T(8,128)} %down_ref.1, ...), custom_call_target="tpu_custom_call" | custom-call | bytes 1000000000 | tf_op jit(solution)/shard_map/pallas_call | solution.py:323
  447.5 0.0 copy-start
  447.5 2.3 copy-done
  449.7 29.2 %shard_map.103 = (bf16[4,2048,896]{2,1,0:T(8,128)(2,1)}, bf16[4,2048,896]{2,1,0:T(8,128)(2,1)}, bf16[4,896,2048]{2,1,0:T(8,128)(2,1)}, bf16[8,128,2048]{2,1,0:T(8,128)(2,1)S(1)}) custom-call(bf16[4,8,32,2176]{3,2,1,0:T(8,128)(2,1)S(1)} %copy-done, bf16[4,2048,896]{2,1,0:T(8,128)(2,1)} %get-tuple-element.13.gate_in, ...), custom_call_target="tpu_custom_call" | custom-call | flops 11274289152 | bytes 88080384 | tf_op jit(solution)/shard_map/pallas_call | solution.py:475
  478.9 59.1 %shard_map.104 = bf16[128,2048]{1,0:T(8,128)(2,1)S(1)} custom-call(bf16[2,2,2,2,64,2048]{5,4,3,2,1,0:T(8,128)(2,1)S(1)} %bitcast.5), custom_call_target="tpu_custom_call" | custom-call | tf_op jit(solution)/shard_map/pallas_call | solution.py:603
  538.0 0.8 copy.16
  (7 shorter events, 0.1 us)
Async XLA Ops:
  447.5 2.3 copy-start

commit v2 on v1

--- a/solution.py
+++ b/solution.py
@@ -146,21 +146,21 @@
     pairs = n_fs // 2
     z, y = fs // 2, lax.rem(fs, 2)
 
-    def relay(kind, hop):
+    def relay(kind, hop, e):
         at = {"up": z - hop, "down": z + hop, "over": z - hop, "over_down": z + hop}[kind]
         to = {"up": fs + 2, "down": fs - 2}.get(kind, fs + 1 - 2 * y)
         origin = at * 2 + y
-        here = packed_ref if hop == 0 else pieces.at[:, origin]
+        here = packed_ref.at[e] if hop == 0 else pieces.at[e, origin]
         slot = ["up", "down", "over", "over_down"].index(kind)
         return pltpu.make_async_remote_copy(
-            here, pieces.at[:, origin], p_send.at[slot, hop], p_recv.at[origin],
+            here, pieces.at[e, origin], p_send.at[slot, hop, e], p_recv.at[origin, e],
             device_id=(gr, to, tp), device_id_type=MESH,
         )
 
-    def landed(origin):
-        piece = pieces.at[:, origin]
-        return pltpu.make_async_remote_copy(
-            piece, piece, p_send.at[0, 0], p_recv.at[origin],
+    def landed(origin, e):
+        piece = pieces.at[e, origin]
+        return pltpu.make_async_remote_copy(
+            piece, piece, p_send.at[0, 0, e], p_recv.at[origin, e],
             device_id=(gr, fs + 1 - 2 * y, tp), device_id_type=MESH,
         )
 
@@ -171,25 +171,26 @@
             return (z + hop < pairs) & (z >= 1)
         return z - hop >= 0 if kind == "over" else z + hop < pairs
 
-    def relay_start(kind, hop):
+    def relay_start(kind, hop, e):
         @pl.when(relayed(kind, hop))
         def _():
-            relay(kind, hop).start()
+            relay(kind, hop, e).start()
 
     def relay_from(hop):
-        @pl.when(z - hop >= 0)
-        def _():
-            landed((z - hop) * 2 + y).wait_recv()
-            relay(kind="over", hop=hop).start()
-
-        relay_start("up", hop)
-
-        @pl.when(z + hop < pairs)
-        def _():
-            landed((z + hop) * 2 + y).wait_recv()
-            relay(kind="over_down", hop=hop).start()
-
-        relay_start("down", hop)
+        for e in range(experts):
+            @pl.when(z - hop >= 0)
+            def _():
+                landed((z - hop) * 2 + y, e).wait_recv()
+
+            relay_start("up", hop, e)
+            relay_start("over", hop, e)
+
+            @pl.when(z + hop < pairs)
+            def _():
+                landed((z + hop) * 2 + y, e).wait_recv()
+
+            relay_start("down", hop, e)
+            relay_start("over_down", hop, e)
 
     own_piece = pltpu.make_async_copy(packed_ref, pieces.at[:, fs], p_own)
 
@@ -199,11 +200,14 @@
         load_down(0, o).start()
     pl.semaphore_wait(barrier, peers)
     for kind in ("up", "down", "over"):
-        relay_start(kind, 0)
+        for e in range(experts):
+            relay_start(kind, 0, e)
     own_piece.start()
 
-    def cast(e):
+    def cast(e, leg):
         for w, o in order:
+            if (o > 0) != (leg == "tp"):
+                continue
             load(e, w, o).wait()
             stage[w, o, e] = (raw[w, o] * gain_ref[...]).astype(BF16)
 
@@ -222,15 +226,16 @@
             for o in range(1, n_tp):
                 fan(e, w, o)
 
-    cast(0)
+    cast(0, "tp")
+    for hop in range(1, pairs):
+        relay_from(hop)
+    cast(0, "fs")
 
     @pl.loop(1, experts)
     def _(e):
-        cast(e)
+        cast(e, "tp")
+        cast(e, "fs")
         forward(e - 1)
-
-    for hop in range(1, pairs):
-        relay_from(hop)
 
     @pl.loop(0, experts)
     def _(e):
@@ -303,12 +308,14 @@
 
     own_piece.wait()
     for at in range(pairs):
-        landed(at * 2 + 1 - y).wait_recv()
+        for e in range(experts):
+            landed(at * 2 + 1 - y, e).wait_recv()
     for kind in ("up", "down", "over", "over_down"):
         for hop in range(1 if kind == "over_down" else 0, pairs):
             @pl.when(relayed(kind, hop))
             def _():
-                relay(kind, hop).wait_send()
+                for e in range(experts):
+                    relay(kind, hop, e).wait_send()
 
 
 def exchange(sizes, norm_gain, gate_master, up_master, down_master, packed):
@@ -350,8 +357,8 @@
             dma((experts,)),
             dma((experts, n_tp, n_gr - 1)),
             dma((experts, n_tp, n_gr - 1)),
-            dma((4, n_fs // 2)),
-            dma((n_fs,)),
+            dma((4, n_fs // 2, experts)),
+            dma((n_fs, experts)),
             dma,
         ],
         compiler_params=pltpu.CompilerParams(

time: 539 us -> 442 us (0.82)
  Pallas kernels: 529 us -> 431 us
    pallas_call x1, Pallas kernels: 441 us -> 343 us  [exchange(): pl.pallas_call(functools.partial(exchange_kernel, n_gr, n_fs, n_tp), out_...]
where the time goes in v2:
time: 442 us; the launch traced here: 441 us
  Pallas kernels  431 us (98%)
    pallas_call x1, Pallas kernels, exchange(): pl.pallas_call(functools.partial(exchange_kernel, n_gr, n_fs, n_tp), out_...  343 us
    pallas_call x1, Pallas kernels, combine(): pl.pallas_call(functools.partial(combine_kernel, n_fs, chunks), out_shape...  59.5 us
    pallas_call x1, Pallas kernels, run_experts(): pl.pallas_call(functools.partial(experts_kernel, slices, 2 * slices), out...  29.2 us

profile of v2, /device:TPU:0, one launch (start us, length us, event | category | flops | bytes accessed | tf_op | source)
XLA Modules:
  0.0 441.2 jit_solution(16021924402608877099)
XLA Ops:
  0.6 0.8 compare_reduce_fusion
  1.4 1.2 fusion
  2.6 0.8 add_divide_fusion.1
  3.4 0.8 fusion.9
  4.2 0.3 reduce_window_sum.11
  4.5 0.8 copy.14.gain_ref
  5.3 1.4 convolution_convert_fusion
  6.8 342.7 %shard_map.102 = (bf16[4,2048,896]{2,1,0:T(8,128)(2,1)}, bf16[4,2048,896]{2,1,0:T(8,128)(2,1)}, bf16[4,896,2048]{2,1,0:T(8,128)(2,1)}, bf16[4,8,32,2176]{3,2,1,0:T(8,128)(2,1)}) custom-call(f32[128,1]{1,0:T(8,128)S(1)} %copy.14.gain_ref, f32[8,128,3584]{2,1,0:T(8,128)} %gate_ref.1, f32[8,128,3584]{2,1,0:T(8,128)} %up_ref.1, f32[8,896,512]{2,1,0:T(8,128)} %down_ref.1, ...), custom_call_target="tpu_custom_call" | custom-call | bytes 1000000000 | tf_op jit(solution)/shard_map/pallas_call | solution.py:330
  349.5 0.0 copy-start
  349.5 2.3 copy-done
  351.8 29.2 %shard_map.103 = (bf16[4,2048,896]{2,1,0:T(8,128)(2,1)}, bf16[4,2048,896]{2,1,0:T(8,128)(2,1)}, bf16[4,896,2048]{2,1,0:T(8,128)(2,1)}, bf16[8,128,2048]{2,1,0:T(8,128)(2,1)S(1)}) custom-call(bf16[4,8,32,2176]{3,2,1,0:T(8,128)(2,1)S(1)} %copy-done, bf16[4,2048,896]{2,1,0:T(8,128)(2,1)} %get-tuple-element.13.gate_in, ...), custom_call_target="tpu_custom_call" | custom-call | flops 11274289152 | bytes 88080384 | tf_op jit(solution)/shard_map/pallas_call | solution.py:482
  380.9 59.5 %shard_map.104 = bf16[128,2048]{1,0:T(8,128)(2,1)S(1)} custom-call(bf16[2,2,2,2,64,2048]{5,4,3,2,1,0:T(8,128)(2,1)S(1)} %bitcast.5), custom_call_target="tpu_custom_call" | custom-call | tf_op jit(solution)/shard_map/pallas_call | solution.py:610
  440.4 0.8 copy.16
  (7 shorter events, 0.1 us)
Async XLA Ops:
  349.5 2.3 copy-start

commit v3 on v2

--- a/solution.py
+++ b/solution.py
@@ -22,7 +22,7 @@
     stage, stage_down, crossed, raw, raw_down,
     load_sem, load_down_sem, x_send, x_recv, s_send, s_recv, own_sem,
     d_send, d_recv, xd_send, xd_recv, own_down_sem, dd_send, dd_recv,
-    p_send, p_recv, p_own,
+    p_send, p_recv, p_own, q_send, q_recv,
 ):
     gr, fs, tp = (lax.axis_index(name) for name in ("gr", "fs", "tp"))
     experts, _, width = gate_out.shape
@@ -146,19 +146,25 @@
     pairs = n_fs // 2
     z, y = fs // 2, lax.rem(fs, 2)
 
+    depth = packed_ref.shape[0] // experts
+    share = packed_ref.shape[1] - packed_ref.shape[0]
+
+    def strip(e):
+        return pl.ds(e * depth, depth)
+
     def relay(kind, hop, e):
         at = {"up": z - hop, "down": z + hop, "over": z - hop, "over_down": z + hop}[kind]
         to = {"up": fs + 2, "down": fs - 2}.get(kind, fs + 1 - 2 * y)
         origin = at * 2 + y
-        here = packed_ref.at[e] if hop == 0 else pieces.at[e, origin]
+        here = packed_ref.at[strip(e)] if hop == 0 else pieces.at[tp, origin, strip(e)]
         slot = ["up", "down", "over", "over_down"].index(kind)
         return pltpu.make_async_remote_copy(
-            here, pieces.at[e, origin], p_send.at[slot, hop, e], p_recv.at[origin, e],
+            here, pieces.at[tp, origin, strip(e)], p_send.at[slot, hop, e], p_recv.at[origin, e],
             device_id=(gr, to, tp), device_id_type=MESH,
         )
 
     def landed(origin, e):
-        piece = pieces.at[e, origin]
+        piece = pieces.at[tp, origin, strip(e)]
         return pltpu.make_async_remote_copy(
             piece, piece, p_send.at[0, 0, e], p_recv.at[origin, e],
             device_id=(gr, fs + 1 - 2 * y, tp), device_id_type=MESH,
@@ -192,7 +198,14 @@
             relay_start("down", hop, e)
             relay_start("over_down", hop, e)
 
-    own_piece = pltpu.make_async_copy(packed_ref, pieces.at[:, fs], p_own)
+    own_piece = pltpu.make_async_copy(packed_ref, pieces.at[tp, fs], p_own)
+
+    def across(origin, side):
+        part = pieces.at[side, origin, :, pl.ds(0, share)]
+        return pltpu.make_async_remote_copy(
+            part, part, q_send.at[origin], q_recv.at[origin],
+            device_id=(gr, fs, tp_at(1)), device_id_type=MESH,
+        )
 
     for w, o in order:
         load(0, w, o).start()
@@ -237,6 +250,15 @@
         cast(e, "fs")
         forward(e - 1)
 
+    own_piece.wait()
+    for at in range(pairs):
+        for e in range(experts):
+            landed(at * 2 + 1 - y, e).wait_recv()
+
+    @pl.loop(0, n_fs)
+    def _(origin):
+        across(origin, tp).start()
+
     @pl.loop(0, experts)
     def _(e):
         for o in [*range(1, n_tp), 0]:
@@ -306,10 +328,11 @@
                 down_over_gr(e, s, o, gr).wait_send()
                 down_over_gr(e, s, o, lax.rem(gr - o + n_gr, n_gr)).wait_recv()
 
-    own_piece.wait()
-    for at in range(pairs):
-        for e in range(experts):
-            landed(at * 2 + 1 - y, e).wait_recv()
+    @pl.loop(0, n_fs)
+    def _(origin):
+        across(origin, tp).wait_send()
+        across(origin, 1 - tp).wait_recv()
+
     for kind in ("up", "down", "over", "over_down"):
         for hop in range(1 if kind == "over_down" else 0, pairs):
             @pl.when(relayed(kind, hop))
@@ -333,7 +356,7 @@
             up_shape,
             up_shape,
             jax.ShapeDtypeStruct((experts, hidden, down_cols * n_gr * n_tp), BF16),
-            jax.ShapeDtypeStruct((packed.shape[0], n_fs, *packed.shape[1:]), BF16),
+            jax.ShapeDtypeStruct((n_tp, n_fs, *packed.shape), BF16),
         ),
         in_specs=[pl.BlockSpec(memory_space=pltpu.VMEM), *[any_spec] * 4],
         out_specs=(any_spec,) * 4,
@@ -360,6 +383,8 @@
             dma((4, n_fs // 2, experts)),
             dma((n_fs, experts)),
             dma,
+            dma((n_fs,)),
+            dma((n_fs,)),
         ],
         compiler_params=pltpu.CompilerParams(
             collective_id=0, has_side_effects=True, vmem_limit_bytes=52 * 1024 * 1024
@@ -370,9 +395,9 @@
 
 def experts_kernel(
     slices, lead,
-    pieces, gate_in, up_in, down_in,
+    blocks, gate_in, up_in, down_in,
     gate_out, up_out, down_out, sums,
-    tall, wide, partial, gate_act, up_act, hidden,
+    tall, wide, pieces, partial, gate_act, up_act, hidden,
     tall_load, tall_store, wide_load, wide_store,
 ):
     experts, features, width = gate_in.shape
@@ -410,6 +435,18 @@
     for j in range(lead):
         load_tall(j // steps, j % steps).start()
 
+    tp = lax.axis_index("tp")
+    share = blocks.shape[3] - tokens
+
+    @pl.loop(0, owners)
+    def _(o):
+        picker = (blocks[tp, o, :, pl.ds(share, tokens)].astype(jnp.float32) > 0).astype(BF16)
+        for side in range(blocks.shape[0]):
+            rows = jnp.dot(
+                picker, blocks[side, o, :, pl.ds(0, share)], preferred_element_type=jnp.float32
+            ).astype(BF16)
+            pieces[:, o, :, pl.ds(side * share, share)] = rows.reshape(experts, -1, share)
+
     @pl.loop(0, experts)
     def _(e):
         for j in range(steps):
@@ -457,7 +494,7 @@
             partial[e] = value.astype(BF16).reshape(partial.shape[1:])
 
         for o in range(owners):
-            weights = pieces[:, o, :, pl.ds(features, tokens)].reshape(-1, tokens)
+            weights = blocks[tp, o, :, pl.ds(share, tokens)]
             rows = partial[:, o].reshape(-1, cols)
             sums[o, :, span(c)] = lax.dot_general(
                 weights, rows, (((0,), (0,)), ((), ())), preferred_element_type=jnp.float32
@@ -471,27 +508,29 @@
             store_wide(c, e).wait()
 
 
-def run_experts(pieces, gate, up, down):
+def run_experts(blocks, gate, up, down):
     experts, features, width = gate.shape
-    _, owners, cap, padded = pieces.shape
-    tokens, count, slices = padded - features, owners * cap, 4
+    _, owners, tokens, _ = blocks.shape
+    cap, slices = tokens // experts, 4
+    count = owners * cap
     ring = 2 * 2 * slices
     any_spec = pl.BlockSpec(memory_space=pl.ANY)
     vmem = pl.BlockSpec(memory_space=pltpu.VMEM)
     dma = pltpu.SemaphoreType.DMA
     return pl.pallas_call(
-        functools.partial(experts_kernel, slices, 2 * slices),
+        functools.partial(experts_kernel, slices, 3 * slices),
         out_shape=(
             jax.ShapeDtypeStruct(gate.shape, BF16),
             jax.ShapeDtypeStruct(up.shape, BF16),
             jax.ShapeDtypeStruct(down.shape, BF16),
-            jax.ShapeDtypeStruct((owners, tokens, features), BF16),
+            pltpu.VMEM((owners, tokens, features), BF16),
         ),
         in_specs=[vmem, any_spec, any_spec, any_spec],
         out_specs=(any_spec, any_spec, any_spec, vmem),
         scratch_shapes=[
             pltpu.VMEM((ring, features // slices, width), BF16),
             pltpu.VMEM((slices * experts, width, features // slices), BF16),
+            pltpu.VMEM((experts, owners, cap, features), BF16),
             pltpu.VMEM((experts, owners, cap, features // slices), BF16),
             pltpu.VMEM((count, width), jnp.float32),
             pltpu.VMEM((count, width), jnp.float32),
@@ -501,12 +540,12 @@
             dma((slices * experts,)),
             dma((slices * experts,)),
         ],
-        compiler_params=pltpu.CompilerParams(vmem_limit_bytes=44 * 1024 * 1024),
+        compiler_params=pltpu.CompilerParams(vmem_limit_bytes=50 * 1024 * 1024),
         cost_estimate=pl.CostEstimate(
             flops=6 * experts * count * features * width,
             bytes_accessed=12 * experts * features * width, transcendentals=0,
         ),
-    )(pieces, gate, up, down)
+    )(blocks, gate, up, down)
 
 
 def plan_of(n_bits, features):
@@ -516,7 +555,7 @@
     units = features // unit
     shares, chunks, begin = [], [], 0
     for i in range(6):
-        shares.append((units - sum(shares)) // (6 - i))
+        shares.append(-((sum(shares) - units) // (6 - i)))
     for i, share in enumerate(shares):
         if share:
             chunks.append((orders[i % 3], begin * unit, share * unit))
@@ -702,16 +741,15 @@
     slot_rank = jnp.cumsum(chosen.astype(jnp.int32), axis=1) - 1
     slot_ids = jnp.arange(CAP, dtype=jnp.int32)
     picker = chosen[:, None, :] & (slot_rank[:, None, :] == slot_ids[None, :, None])
-    packed = jnp.einsum(
-        "xsr,rd->xsd", picker.astype(jnp.bfloat16), normed, preferred_element_type=jnp.float32
-    ).astype(jnp.bfloat16)
     combiner = (picker.astype(jnp.float32) * weight_rows[:, None, :]).astype(jnp.bfloat16)
-    gate_moved, up_moved, down_moved, pieces = exchange(
+    share = tokens.shape[1] // n_tp
+    strip = lax.dynamic_slice_in_dim(normed, lax.axis_index("tp") * share, share, axis=1)
+    gate_moved, up_moved, down_moved, blocks = exchange(
         sizes, norm_gain, gate_master, up_master, down_master,
-        jnp.concatenate([packed, combiner], axis=2),
+        jnp.concatenate([strip, combiner.reshape(-1, tokens.shape[0])], axis=1),
     )
     gate_weight, up_weight, down_weight, sums = run_experts(
-        pieces, gate_moved, up_moved, down_moved
+        blocks, gate_moved, up_moved, down_moved
     )
     return (gate_weight, up_weight, down_weight, combine(n_fs, sums))
 
@@ -733,6 +771,7 @@
         aligned = width % 128 == 0 and down_master.shape[2] % 128 == 0
         fits = n_fs % n_tp == 0 and n_fs & (n_fs - 1) == 0 and n_fs > 2
         fits = fits and n_gr > 1 and n_tp == 2 and tokens.shape[0] % 128 == 0
+        fits = fits and gate_master.shape[0] // n_tp * CAP == tokens.shape[0]
         run = functools.partial(fast_local, (n_gr, n_fs, n_tp)) if aligned and fits else plain_local
         return run(tokens, route_ids, route_logits, norm_gain, gate_master, up_master, down_master)
 

time: 442 us -> 429 us (0.971)
  Pallas kernels: 431 us -> 421 us
    pallas_call x1, Pallas kernels: 343 us -> 332 us  [exchange(): pl.pallas_call(functools.partial(exchange_kernel, n_gr, n_fs, n_tp), out_...]
where the time goes in v3:
time: 429 us
  Pallas kernels  421 us (98%)
  other arithmetic  5.21 us (1%)
    pallas_call x1, Pallas kernels, exchange(): pl.pallas_call(functools.partial(exchange_kernel, n_gr, n_fs, n_tp), out_...  332 us
    pallas_call x1, Pallas kernels, combine(): pl.pallas_call(functools.partial(combine_kernel, n_fs, chunks), out_shape...  58.2 us
    pallas_call x1, Pallas kernels, run_experts(): pl.pallas_call(functools.partial(experts_kernel, slices, 3 * slices), out...  31.3 us

profile of v3, /device:TPU:0, one launch (start us, length us, event | category | flops | bytes accessed | tf_op | source)
XLA Modules:
  0.0 428.9 jit_solution(2720906837769977815)
XLA Ops:
  0.6 0.8 compare_reduce_fusion
  1.4 1.2 multiply_reduce_fusion
  2.6 0.8 add_divide_fusion.1
  3.4 0.8 fusion.3
  4.2 0.3 reduce_window_sum.11
  4.5 0.1 eq.39
  4.6 0.1 fusion.1
  4.7 0.8 copy.14.gain_ref
  5.5 1.1 convert_element_type.18
  6.6 0.1 fusion
  6.7 331.8 %shard_map.102 = (bf16[4,2048,896]{2,1,0:T(8,128)(2,1)}, bf16[4,2048,896]{2,1,0:T(8,128)(2,1)}, bf16[4,896,2048]{2,1,0:T(8,128)(2,1)}, bf16[2,8,128,1152]{3,2,1,0:T(8,128)(2,1)}) custom-call(f32[128,1]{1,0:T(8,128)S(1)} %copy.14.gain_ref, f32[8,128,3584]{2,1,0:T(8,128)} %gate_ref.1, f32[8,128,3584]{2,1,0:T(8,128)} %up_ref.1, f32[8,896,512]{2,1,0:T(8,128)} %down_ref.1, ...), custom_call_target="tpu_custom_call" | custom-call | bytes 1000000000 | tf_op jit(solution)/shard_map/pallas_call | solution.py:353
  338.6 31.3 %shard_map.103 = (bf16[4,2048,896]{2,1,0:T(8,128)(2,1)}, bf16[4,2048,896]{2,1,0:T(8,128)(2,1)}, bf16[4,896,2048]{2,1,0:T(8,128)(2,1)}, bf16[8,128,2048]{2,1,0:T(8,128)(2,1)S(1)}) custom-call(bf16[2,8,128,1152]{3,2,1,0:T(8,128)(2,1)} %get-tuple-element.12.blocks, bf16[4,2048,896]{2,1,0:T(8,128)(2,1)} %get-tuple-element.13.gate_in, ...), custom_call_target="tpu_custom_call" | custom-call | flops 11274289152 | bytes 88080384 | tf_op jit(solution)/shard_map/pallas_call | solution.py:520
  369.9 58.2 %shard_map.104 = bf16[128,2048]{1,0:T(8,128)(2,1)S(1)} custom-call(bf16[2,2,2,2,64,2048]{5,4,3,2,1,0:T(8,128)(2,1)S(1)} %bitcast.14), custom_call_target="tpu_custom_call" | custom-call | tf_op jit(solution)/shard_map/pallas_call | solution.py:649
  428.1 0.8 copy.16
  (7 shorter events, 0.1 us)

commit v4 on v3

--- a/solution.py
+++ b/solution.py
@@ -13,6 +13,47 @@
 epsilon = 1e-06
 MESH = pl.DeviceIdType.MESH
 BF16 = jnp.bfloat16
+
+
+def prepare_kernel(per_plane, tokens_ref, ids_ref, logits_ref, gain_ref, piece, gain_out):
+    rows, share = tokens_ref.shape[0], piece.shape[1] - tokens_ref.shape[0]
+    tp = lax.axis_index("tp")
+    values = tokens_ref[...].astype(jnp.float32)
+    scale = lax.rsqrt(jnp.mean(values * values, axis=-1, keepdims=True) + epsilon)
+    half = tokens_ref[:, pl.ds(pl.multiple_of(tp * share, share), share)]
+    piece[:, pl.ds(0, share)] = (half.astype(jnp.float32) * scale).astype(BF16)
+
+    down = lax.broadcasted_iota(jnp.int32, (rows, rows), 0)
+    right = lax.broadcasted_iota(jnp.int32, (rows, rows), 1)
+
+    def column(line):
+        return jnp.sum(jnp.where(down == right, line, 0.0), axis=1, keepdims=True)
+
+    gain_out[...] = column(gain_ref[...])
+    ids = ids_ref[...].astype(jnp.float32)
+    differ = column(logits_ref[0:1, :] - logits_ref[1:2, :])
+    expert = (right // CAP + tp * per_plane).astype(jnp.float32)
+    first, second = column(ids[0:1, :]) == expert, column(ids[1:2, :]) == expert
+    weight = jnp.where(first, jax.nn.sigmoid(differ), 0.0)
+    weight = weight + jnp.where(second, jax.nn.sigmoid(-differ), 0.0)
+    hits = jnp.where(first | second, 1.0, 0.0)
+    upto = jnp.where(right <= down, 1.0, 0.0).astype(BF16)
+    rank = jnp.dot(upto, hits.astype(BF16), preferred_element_type=jnp.float32)
+    slot = (right % CAP + 1).astype(jnp.float32)
+    kept = jnp.where(rank == slot, hits * weight, 0.0)
+    piece[:, pl.ds(share, rows)] = kept.astype(BF16)
+
+
+def prepare(n_tp, experts, tokens, route_ids, route_logits, norm_gain):
+    rows, features = tokens.shape
+    return pl.pallas_call(
+        functools.partial(prepare_kernel, experts),
+        out_shape=(
+            pltpu.VMEM((rows, features // n_tp + rows), BF16),
+            pltpu.VMEM((norm_gain.shape[0], 1), jnp.float32),
+        ),
+        name="prepare",
+    )(tokens, route_ids.T, route_logits.T, norm_gain[None, :])
 
 
 def exchange_kernel(
@@ -341,7 +382,7 @@
                     relay(kind, hop, e).wait_send()
 
 
-def exchange(sizes, norm_gain, gate_master, up_master, down_master, packed):
+def exchange(sizes, gain, gate_master, up_master, down_master, packed):
     n_gr, n_fs, n_tp = sizes
     all_experts, rows, cols = gate_master.shape
     experts = all_experts // n_tp
@@ -390,7 +431,7 @@
             collective_id=0, has_side_effects=True, vmem_limit_bytes=52 * 1024 * 1024
         ),
         cost_estimate=pl.CostEstimate(flops=0, bytes_accessed=1_000_000_000, transcendentals=0),
-    )(norm_gain[:, None], gate_master, up_master, down_master, packed)
+    )(gain, gate_master, up_master, down_master, packed)
 
 
 def experts_kernel(
@@ -442,8 +483,9 @@
     def _(o):
         picker = (blocks[tp, o, :, pl.ds(share, tokens)].astype(jnp.float32) > 0).astype(BF16)
         for side in range(blocks.shape[0]):
-            rows = jnp.dot(
-                picker, blocks[side, o, :, pl.ds(0, share)], preferred_element_type=jnp.float32
+            rows = lax.dot_general(
+                picker, blocks[side, o, :, pl.ds(0, share)], (((0,), (0,)), ((), ())),
+                preferred_element_type=jnp.float32,
             ).astype(BF16)
             pieces[:, o, :, pl.ds(side * share, share)] = rows.reshape(experts, -1, share)
 
@@ -496,8 +538,8 @@
         for o in range(owners):
             weights = blocks[tp, o, :, pl.ds(share, tokens)]
             rows = partial[:, o].reshape(-1, cols)
-            sums[o, :, span(c)] = lax.dot_general(
-                weights, rows, (((0,), (0,)), ((), ())), preferred_element_type=jnp.float32
+            sums[o, :, span(c)] = jnp.dot(
+                weights, rows, preferred_element_type=jnp.float32
             ).astype(BF16)
 
     for i in range(ring):
@@ -726,27 +768,11 @@
 
 def fast_local(sizes, tokens, route_ids, route_logits, norm_gain, gate_master, up_master, down_master):
     n_gr, n_fs, n_tp = sizes
-    as_float = tokens.astype(jnp.float32)
-    normed = (
-        as_float * lax.rsqrt(jnp.mean(as_float * as_float, axis=-1, keepdims=True) + epsilon)
-    ).astype(jnp.bfloat16)
-    differ = route_logits[:, 0] - route_logits[:, 1]
-    route_weight = jnp.stack([jax.nn.sigmoid(differ), jax.nn.sigmoid(-differ)], axis=1)
-    experts_here = gate_master.shape[0] // n_tp
-    first_expert = lax.axis_index("tp") * experts_here
-    expert_ids = first_expert + jnp.arange(experts_here, dtype=jnp.int32)
-    route_hits = route_ids[None, :, :] == expert_ids[:, None, None]
-    chosen = jnp.any(route_hits, axis=2)
-    weight_rows = jnp.sum(jnp.where(route_hits, route_weight[None, :, :], 0.0), axis=2)
-    slot_rank = jnp.cumsum(chosen.astype(jnp.int32), axis=1) - 1
-    slot_ids = jnp.arange(CAP, dtype=jnp.int32)
-    picker = chosen[:, None, :] & (slot_rank[:, None, :] == slot_ids[None, :, None])
-    combiner = (picker.astype(jnp.float32) * weight_rows[:, None, :]).astype(jnp.bfloat16)
-    share = tokens.shape[1] // n_tp
-    strip = lax.dynamic_slice_in_dim(normed, lax.axis_index("tp") * share, share, axis=1)
+    packed, gain = prepare(
+        n_tp, gate_master.shape[0] // n_tp, tokens, route_ids, route_logits, norm_gain
+    )
     gate_moved, up_moved, down_moved, blocks = exchange(
-        sizes, norm_gain, gate_master, up_master, down_master,
-        jnp.concatenate([strip, combiner.reshape(-1, tokens.shape[0])], axis=1),
+        sizes, gain, gate_master, up_master, down_master, packed
     )
     gate_weight, up_weight, down_weight, sums = run_experts(
         blocks, gate_moved, up_moved, down_moved
@@ -772,6 +798,7 @@
         fits = n_fs % n_tp == 0 and n_fs & (n_fs - 1) == 0 and n_fs > 2
         fits = fits and n_gr > 1 and n_tp == 2 and tokens.shape[0] % 128 == 0
         fits = fits and gate_master.shape[0] // n_tp * CAP == tokens.shape[0]
+        fits = fits and norm_gain.shape[0] == tokens.shape[0]
         run = functools.partial(fast_local, (n_gr, n_fs, n_tp)) if aligned and fits else plain_local
         return run(tokens, route_ids, route_logits, norm_gain, gate_master, up_master, down_master)
 

time: 429 us -> 424 us (0.988)
  other arithmetic: 5.21 us -> 0 us
where the time goes in v4:
time: 424 us
  Pallas kernels  423 us (100%)
    pallas_call x1, Pallas kernels, exchange(): pl.pallas_call(functools.partial(exchange_kernel, n_gr, n_fs, n_tp), out_...  332 us
    pallas_call x1, Pallas kernels, combine(): pl.pallas_call(functools.partial(combine_kernel, n_fs, chunks), out_shape...  58 us
    pallas_call x1, Pallas kernels, run_experts(): pl.pallas_call(functools.partial(experts_kernel, slices, 3 * slices), out...  31.5 us

profile of v4, /device:TPU:0, one launch (start us, length us, event | category | flops | bytes accessed | tf_op | source)
XLA Modules:
  0.0 424.1 jit_solution(1562856696205098906)
XLA Ops:
  0.6 1.3 prepare.1
  2.0 331.8 %shard_map.102 = (bf16[4,2048,896]{2,1,0:T(8,128)(2,1)}, bf16[4,2048,896]{2,1,0:T(8,128)(2,1)}, bf16[4,896,2048]{2,1,0:T(8,128)(2,1)}, bf16[2,8,128,1152]{3,2,1,0:T(8,128)(2,1)}) custom-call(f32[128,1]{1,0:T(8,128)S(1)} %get-tuple-element.14.gain_ref, f32[8,128,3584]{2,1,0:T(8,128)} %gate_ref.1, f32[8,128,3584]{2,1,0:T(8,128)} %up_ref.1, ...), custom_call_target="tpu_custom_call" | custom-call | bytes 1000000000 | tf_op jit(solution)/shard_map/pallas_call | solution.py:394
  333.8 31.5 %shard_map.103 = (bf16[4,2048,896]{2,1,0:T(8,128)(2,1)}, bf16[4,2048,896]{2,1,0:T(8,128)(2,1)}, bf16[4,896,2048]{2,1,0:T(8,128)(2,1)}, bf16[8,128,2048]{2,1,0:T(8,128)(2,1)S(1)}) custom-call(bf16[2,8,128,1152]{3,2,1,0:T(8,128)(2,1)} %get-tuple-element.16.blocks, bf16[4,2048,896]{2,1,0:T(8,128)(2,1)} %get-tuple-element.17.gate_in, ...), custom_call_target="tpu_custom_call" | custom-call | flops 11274289152 | bytes 88080384 | tf_op jit(solution)/shard_map/pallas_call | solution.py:562
  365.3 58.0 %shard_map.104 = bf16[128,2048]{1,0:T(8,128)(2,1)S(1)} custom-call(bf16[2,2,2,2,64,2048]{5,4,3,2,1,0:T(8,128)(2,1)S(1)} %bitcast.4), custom_call_target="tpu_custom_call" | custom-call | tf_op jit(solution)/shard_map/pallas_call | solution.py:691
  423.3 0.8 copy.12
